TPU v7x, 32 devices: a whole 2x2x4 slice. The times are simulated.
32 devices in a mesh: ep: 16 (over z, y, core), tp: 2 (over x).
Axes of the slice: x: 2, y: 2, z: 4, core: 2. Of those that a mesh axis runs over, the one named last changes fastest.
Arguments:
- tokens: bfloat16 [128, 1024], P(('ep', 'tp')), may hold values from -6 to 6
- lengths: int32 [128], P('ep'), may hold values from 256 to 1024
- key_cache: bfloat16 [128, 1024, 128], P(('ep', 'tp')), may hold values from -1500 to 1500
- value_cache: bfloat16 [128, 1024, 128], P(('ep', 'tp')), may hold values from -6 to 6
- query_weight: bfloat16 [1024, 512], P(None, 'tp'), may hold values from -0.1875 to 0.1875
- key_weight: bfloat16 [1024, 128], replicated, may hold values from -0.1875 to 0.1875
- value_weight: bfloat16 [1024, 128], replicated, may hold values from -0.1875 to 0.1875
- lambdas: float32 [4], replicated, may hold values from 0.3 to 0.8
- head_gain: float32 [128], replicated, may hold values from 0.1 to 1.9
- output_weight: bfloat16 [512, 1024], P(None, 'tp'), may hold values from -0.25 to 0.25
- norm1_gain: float32 [1024], replicated, may hold values from 0.1 to 1.9
- routes: int32 [128, 6], P('ep'), may hold values from 0 to 15, all different within a row; in each aligned block of 8 rows (0 to 7, 8 to 15, ...) at most 6 rows name the same one
- route_logits: float32 [128, 6], P('ep'), may hold values from -9 to 410
- gate_weight: bfloat16 [16, 1024, 1024], P('ep', None, 'tp'), may hold values from -0.5 to 0.5
- up_weight: bfloat16 [16, 1024, 1024], P('ep', None, 'tp'), may hold values from -0.5 to 0.5
- down_weight: bfloat16 [16, 1024, 1024], P('ep', 'tp'), may hold values from -0.09375 to 0.09375
- norm2_gain: float32 [1024], replicated, may hold values from 0.1 to 1.9
Outputs:
- mixed: bfloat16 [128, 1024], P('ep', 'tp')
Inputs may be any that keep to these rules, and one draw needn't show every extreme that they name: `routes`: in the 8 rows of each aligned block (the rows held by one index of ep) no expert is named by more than 6 rows, a bound that some block reaches; the experts of a row differ.
All inputs are finite; a program needn't handle non-finite values.
Results may differ from a plain program's by a relative error of at most 0.014.
Values may be sent and summed in bfloat16 or wider, within the bound.
No kernel may reach another device: no remote copies, remote signals or barrier semaphores. Data moves between devices by JAX's collectives and lax.ppermute only.
A program may use at most 64 MiB of HBM per device.

v0:
```python
import jax
import jax.numpy as jnp
from jax import lax
from jax.sharding import PartitionSpec as P

ALPHA = 1.4142135623730951
EPS = 1e-05
THETA = 500000.0
LIMIT = 7.0
SLOPE = 1.702


def rotate(values, positions):
    half = values.shape[-1] // 2
    freqs = THETA ** (-jnp.arange(half, dtype=jnp.float32) / half)
    angles = positions.astype(jnp.float32)[:, None] * freqs[None, :]
    shape = (angles.shape[0],) + (1,) * (values.ndim - 2) + (half,)
    cosine = jnp.cos(angles).reshape(shape)
    sine = jnp.sin(angles).reshape(shape)
    first = values[..., :half]
    second = values[..., half:]
    return jnp.concatenate(
        [first * cosine - second * sine, second * cosine + first * sine], axis=-1
    )


def scaled_part(summed, sums, squares, width, gain):
    mean = sums / width
    spread = squares / width - mean * mean
    return (summed - mean[:, None]) * lax.rsqrt(spread + EPS)[:, None] * gain


def choose_slots(routes_block, experts, capacity):
    flat = routes_block.reshape(-1)
    onehot = (flat[:, None] == jnp.arange(experts, dtype=jnp.int32)[None, :]).astype(jnp.int32)
    before = jnp.cumsum(onehot, axis=0) - onehot
    slot = jnp.sum(before * onehot, axis=1)
    target = flat * capacity + slot
    return target[:, None] == jnp.arange(experts * capacity, dtype=jnp.int32)[None, :]


def body(
    tokens,
    lengths,
    key_cache,
    value_cache,
    query_weight,
    key_weight,
    value_weight,
    lambdas,
    head_gain,
    output_weight,
    norm1_gain,
    routes,
    route_logits,
    gate_weight,
    up_weight,
    down_weight,
    norm2_gain,
):
    bf16 = jnp.bfloat16
    f32 = jnp.float32
    tp_count = lax.axis_size("tp")
    tp_rank = lax.axis_index("tp")
    own, width = tokens.shape
    group = own * tp_count
    part = width // tp_count
    heads = lambdas.shape[0]
    head_dim = key_weight.shape[1] // 2
    length = key_cache.shape[1]
    group_rows = lax.all_gather(tokens, "tp", axis=0, tiled=True)
    query = jnp.dot(group_rows, query_weight, preferred_element_type=f32).reshape(
        group, -1, 2, head_dim
    )
    query = rotate(query, lengths).astype(bf16).reshape(group, -1)
    query = lax.all_to_all(query, "tp", split_axis=0, concat_axis=1, tiled=True).reshape(
        own, heads, 2, head_dim
    )
    own_lengths = lax.dynamic_slice_in_dim(lengths, tp_rank * own, own)
    new_key = jnp.dot(tokens, key_weight, preferred_element_type=f32).reshape(own, 2, head_dim)
    new_key = rotate(new_key, own_lengths).astype(bf16)
    new_value = jnp.dot(tokens, value_weight, preferred_element_type=f32).astype(bf16)
    keys = key_cache.reshape(own, length, 2, head_dim)
    scale = head_dim ** (-0.5)
    past = jnp.einsum("bhmd,bjmd->bhmj", query, keys, preferred_element_type=f32) * scale
    live = jnp.arange(length, dtype=jnp.int32)[None, :] < own_lengths[:, None]
    past = jnp.where(live[:, None, None, :], past, -jnp.inf)
    selfs = jnp.einsum("bhmd,bmd->bhm", query, new_key, preferred_element_type=f32) * scale
    top = jnp.maximum(jnp.max(past, axis=-1), selfs)
    past_exp = jnp.exp(past - top[..., None])
    self_exp = jnp.exp(selfs - top)
    total = jnp.sum(past_exp, axis=-1) + self_exp
    past_prob = past_exp / total[..., None]
    self_prob = self_exp / total
    mixing = lambdas[None, :]
    past_weight = (past_prob[:, :, 0] - mixing[..., None] * past_prob[:, :, 1]).astype(bf16)
    self_weight = (self_prob[:, :, 0] - mixing * self_prob[:, :, 1]).astype(bf16)
    head_out = jnp.einsum("bhj,bje->bhe", past_weight, value_cache, preferred_element_type=f32)
    head_out = head_out + self_weight.astype(f32)[..., None] * new_value.astype(f32)[:, None, :]
    normed = (
        head_out
        * lax.rsqrt(jnp.mean(head_out * head_out, axis=-1, keepdims=True) + EPS)
        * head_gain
    )
    attended = normed.astype(bf16).reshape(own, -1)
    mix = jnp.dot(
        lax.all_gather(attended, "tp", axis=0, tiled=True),
        output_weight,
        preferred_element_type=f32,
    )
    column_start = tp_rank * part
    own_columns = lax.dynamic_slice_in_dim(group_rows, column_start, part, 1).astype(f32)
    summed = ALPHA * own_columns + mix
    sums, squares = lax.psum((jnp.sum(summed, axis=1), jnp.sum(summed * summed, axis=1)), "tp")
    gain_part = lax.dynamic_slice_in_dim(norm1_gain, column_start, part)
    settled_part = scaled_part(summed, sums, squares, width, gain_part).astype(bf16)
    settled = lax.all_gather(settled_part, "tp", axis=1, tiled=True)
    experts = lax.axis_size("ep")
    topk = routes.shape[1]
    capacity = min(group, max(2, 2 * group * topk // experts))
    chosen = choose_slots(routes, experts, capacity)
    placing = jnp.sum(chosen.reshape(group, topk, -1).astype(f32), axis=1).astype(bf16)
    route_weight = jax.nn.softmax(route_logits, axis=-1)
    gate_local = gate_weight[0]
    up_local = up_weight[0]
    down_local = down_weight[0]
    outgoing = lax.dot_general(
        placing, settled, (((0,), (0,)), ((), ())), preferred_element_type=f32
    )
    outgoing = outgoing.astype(bf16).reshape(experts, capacity, width)
    rows = lax.all_to_all(outgoing, "ep", split_axis=0, concat_axis=0, tiled=True)
    gate_h = jnp.einsum("scd,df->scf", rows, gate_local, preferred_element_type=f32)
    up_h = jnp.einsum("scd,df->scf", rows, up_local, preferred_element_type=f32)
    clipped = jnp.minimum(gate_h, LIMIT)
    linear = jnp.clip(up_h, -LIMIT, LIMIT)
    act = (clipped * jax.nn.sigmoid(SLOPE * clipped) * (linear + 1.0)).astype(bf16)
    terms = jnp.einsum("scf,fd->scd", act, down_local, preferred_element_type=f32)
    answers = (
        lax.psum_scatter(terms.astype(jnp.bfloat16), "tp", scatter_dimension=2, tiled=True)
        .astype(jnp.float32)
        .astype(bf16)
    )
    selector = chosen.astype(bf16)
    back = lax.all_to_all(answers, "ep", split_axis=0, concat_axis=0, tiled=True)
    picked = jnp.dot(selector, back.reshape(experts * capacity, -1), preferred_element_type=f32)
    routed = jnp.sum(picked.reshape(group, topk, -1) * route_weight[:, :, None], axis=1)
    final = ALPHA * settled_part.astype(f32) + routed
    sums, squares = lax.psum((jnp.sum(final, axis=1), jnp.sum(final * final, axis=1)), "tp")
    gain_part = lax.dynamic_slice_in_dim(norm2_gain, column_start, part)
    result = scaled_part(final, sums, squares, width, gain_part).astype(bf16)
    return result


def solution(mesh):
    in_specs = (
        P(("ep", "tp"), None),
        P("ep"),
        P(("ep", "tp"), None, None),
        P(("ep", "tp"), None, None),
        P(None, "tp"),
        P(),
        P(),
        P(),
        P(),
        P(None, "tp"),
        P(),
        P("ep", None),
        P("ep", None),
        P("ep", None, "tp"),
        P("ep", None, "tp"),
        P("ep", "tp", None),
        P(),
    )
    out_specs = P("ep", "tp")
    return jax.shard_map(body, mesh=mesh, in_specs=in_specs, out_specs=out_specs, check_vma=False)
```

profile of v0, /device:TPU:0, one launch (start us, length us, event | category | flops | bytes accessed | tf_op | source)
XLA Modules:
  0.0 96.1 jit_solution(3601989085853479555)
XLA Ops:
  6.6 0.7 copy-done.11
  7.3 5.6 %all-gather = bf16[2,4,1024]{2,1,0:T(4,128)(2,1)S(1)} all-gather(bf16[1,4,1024]{2,1,0:T(4,128)(2,1)} %bitcast.75), channel_id=1, replica_groups=mesh['ep'=16,'tp'=2] {'tp'}, dimensions={0}, use_global_device_ids=true | all-gather | bytes 24576 | tf_op jit(solution)/shard_map/all_gather | solution.py:71
  12.9 1.2 %fusion.54 = f32[8,256]{1,0:T(8,128)S(1)} fusion(bf16[8,1024]{1,0:T(8,128)(2,1)S(1)} %reshape.226, bf16[1024,256]{1,0:T(8,128)(2,1)} %param.21), kind=kOutput, calls=%fused_computation.97 | convolution fusion | flops 4194304 | bytes 548864 | tf_op jit(solution)/shard_map/dot_general | solution.py:72
  14.5 0.7 convert_element_type.66
  15.1 3.2 %all-to-all-start = ((bf16[2,4,256]{2,1,0:T(4,128)(2,1)}), bf16[2,4,256]{2,1,0:T(4,128)(2,1)S(1)}, u32[]{:S(2)}, u32[]{:S(2)}) async-start(bf16[2,4,256]{2,1,0:T(4,128)(2,1)} %convert_element_type.66), calls=%async_computation | async-start | bytes 8192 | tf_op jit(solution)/shard_map/all_to_all | solution.py:76
  18.6 1.1 %fusion.55 = f32[4,128]{1,0:T(4,128)S(1)} fusion(bf16[4,1024]{1,0:T(4,128)(2,1)} %param.17, bf16[1024,128]{1,0:T(8,128)(2,1)} %param.22), kind=kOutput, calls=%fused_computation.98 | convolution fusion | flops 1048576 | bytes 272384 | tf_op jit(solution)/shard_map/dot_general | solution.py:80
  19.9 0.8 fusion.6
  21.6 0.5 copy.54
  22.6 0.3 fusion.53
  22.9 0.2 fusion.21
  23.3 0.6 copy-done.8
  24.0 0.4 multiply_reduce_fusion.2
  24.4 0.2 copy-done.12
  24.7 4.3 %all-gather.1 = bf16[2,4,512]{2,1,0:T(4,128)(2,1)S(1)} all-gather(bf16[1,4,512]{2,1,0:T(4,128)(2,1)S(1)} %reshape.227), channel_id=1, replica_groups=mesh['ep'=16,'tp'=2] {'tp'}, dimensions={0}, use_global_device_ids=true | all-gather | bytes 12288 | tf_op jit(solution)/shard_map/all_gather | solution.py:107
  29.1 0.3 fusion.51
  29.4 4.9 %all-reduce.1 = (f32[8]{0:T(128)S(1)}, f32[8]{0:T(128)S(1)}) all-reduce(f32[8]{0:T(128)S(1)} %get-tuple-element.8, f32[8]{0:T(128)S(1)} %get-tuple-element.7), channel_id=1, replica_groups=mesh['ep'=16,'tp'=2] {'tp'}, use_global_device_ids=true, to_apply=%region_6.7 | all-reduce | flops 16 | bytes 128 | tf_op jit(solution)/shard_map/psum | solution.py:114
  34.4 4.4 %all_gather.11 = bf16[8,1024]{1,0:T(8,128)(2,1)S(1)} all-gather(bf16[8,512]{1,0:T(8,128)(2,1)S(1)} %multiply_convert_fusion.1), channel_id=1, replica_groups=mesh['ep'=16,'tp'=2] {'tp'}, dimensions={1}, use_global_device_ids=true | all-gather | bytes 24576 | tf_op jit(solution)/shard_map/all_gather | solution.py:117
  38.8 0.2 convolution_convert_fusion.1
  39.1 16.2 %all_to_all.23 = bf16[16,6,1024]{2,1,0:T(8,128)(2,1)S(1)} all-to-all(bf16[16,6,1024]{2,1,0:T(8,128)(2,1)S(1)} %reshape.222), channel_id=1, replica_groups=mesh['ep'=16,'tp'=2] {'ep'}, dimensions={0} | all-to-all | bytes 393216 | tf_op jit(solution)/shard_map/all_to_all | solution.py:131
  55.4 0.3 convolution_minimum_fusion
  55.7 2.5 %convolution_convert_fusion = bf16[16,6,1024]{2,0,1:T(8,128)(2,1)} fusion(bf16[1,512,1024]{2,1,0:T(8,128)(2,1)S(1)} %copy-done, bf16[1,1024,512]{2,1,0:T(8,128)(2,1)} %param.31, f32[16,6,512]{2,0,1:T(8,128)S(1)} %convolution_minimum_fusion, bf16[16,6,1024]{2,1,0:T(8,128)(2,1)S(1)} %all_to_all.23), kind=kOutput, calls=%fused_computation | convolution fusion | flops 201867264 | bytes 2686976 | tf_op jit(solution)/shard_map/scf,fd->scd/dot_general | solution.py:137
  58.2 0.7 copy-done.6
  59.0 0.2 fusion.42
  59.2 8.9 %reduce-scatter.2.cloned.1.call-done = bf16[16,6,512]{2,0,1:T(8,128)(2,1)} async-done(((bf16[16,6,1024]{2,0,1:T(8,128)(2,1)}), bf16[16,6,512]{2,0,1:T(8,128)(2,1)}) %reduce-scatter.2.cloned.1.call-update) | async-done | bytes 98320 | tf_op jit(solution)/shard_map/reduce_scatter | solution.py:139
  68.0 1.6 %copy.61 = bf16[16,6,512]{2,1,0:T(8,128)(2,1)} copy(bf16[16,6,512]{2,0,1:T(8,128)(2,1)} %reduce-scatter.2.cloned.1.call-done) | data formatting | bytes 196608 | tf_op jit(solution)/shard_map/reduce_scatter | solution.py:139
  69.6 5.6 %all-to-all-start.2 = ((bf16[16,6,512]{2,1,0:T(8,128)(2,1)}), bf16[16,6,512]{2,1,0:T(8,128)(2,1)S(1)}, u32[]{:S(2)}, u32[]{:S(2)}) async-start(bf16[16,6,512]{2,1,0:T(8,128)(2,1)} %copy.61), calls=%async_computation.3 | async-start | bytes 262144 | tf_op jit(solution)/shard_map/all_to_all | solution.py:144
  75.4 0.6 copy-done.10
  76.1 7.1 %all-to-all-done.2 = bf16[16,6,512]{2,1,0:T(8,128)(2,1)S(1)} async-done(((bf16[16,6,512]{2,1,0:T(8,128)(2,1)}), bf16[16,6,512]{2,1,0:T(8,128)(2,1)S(1)}, u32[]{:S(2)}, u32[]{:S(2)}) %all-to-all-start.2) | async-done | bytes 98336 | tf_op jit(solution)/shard_map/all_to_all | solution.py:144
  83.2 0.2 fusion.5
  83.4 0.2 fusion.38
  83.6 4.9 %all-reduce = (f32[8]{0:T(128)S(1)}, f32[8]{0:T(128)S(1)}) all-reduce(f32[8]{0:T(128)S(1)} %get-tuple-element.6, f32[8]{0:T(128)S(1)} %get-tuple-element.5), channel_id=1, replica_groups=mesh['ep'=16,'tp'=2] {'tp'}, use_global_device_ids=true, to_apply=%region_17.18 | all-reduce | flops 16 | bytes 128 | tf_op jit(solution)/shard_map/psum | solution.py:148
  88.6 0.7 multiply_convert_fusion
  (66 shorter events, 2.9 us)
Async XLA Ops:
  6.5 49.2 %copy-start = (bf16[1,512,1024]{2,1,0:T(8,128)(2,1)S(1)}, bf16[1,512,1024]{2,1,0:T(8,128)(2,1)}, u32[]{:S(2)}) copy-start(bf16[1,512,1024]{2,1,0:T(8,128)(2,1)} %param.32) | copy-start | bytes 3145732
  6.5 0.7 copy-start.11
  6.5 13.4 %copy-start.5 = (bf16[1024,128]{1,0:T(8,128)(2,1)S(1)}, bf16[1024,128]{1,0:T(8,128)(2,1)}, u32[]{:S(2)}) copy-start(bf16[1024,128]{1,0:T(8,128)(2,1)} %param.23) | copy-start | bytes 786436
  6.5 15.1 %copy-start.1 = (bf16[4,1024,128]{2,1,0:T(8,128)(2,1)S(1)}, bf16[4,1024,128]{2,1,0:T(8,128)(2,1)}, u32[]{:S(2)}) copy-start(bf16[4,1024,128]{2,1,0:T(8,128)(2,1)} %param.19) | copy-start | bytes 3145732
  15.1 7.2 %all-to-all-start = ((bf16[2,4,256]{2,1,0:T(4,128)(2,1)}), bf16[2,4,256]{2,1,0:T(4,128)(2,1)S(1)}, u32[]{:S(2)}, u32[]{:S(2)}) async-start(bf16[2,4,256]{2,1,0:T(4,128)(2,1)} %convert_element_type.66), calls=%async_computation | async-start | bytes 8192 | tf_op jit(solution)/shard_map/all_to_all | solution.py:76
  18.4 49.7 %reduce-scatter.2.cloned.1.call-start = ((), (), s32[]{:S(2)}) async-start(), calls=%async_computation.4 | async-start | bytes 294912 | tf_op jit(solution)/shard_map/reduce_scatter | solution.py:139
  19.9 0.9 copy-start.7
  21.6 0.7 copy-start.9
  22.1 1.8 %copy-start.2 = (bf16[4,1024,128]{2,1,0:T(8,128)(2,1)S(1)}, bf16[4,1024,128]{2,1,0:T(8,128)(2,1)}, u32[]{:S(2)}) copy-start(bf16[4,1024,128]{2,1,0:T(8,128)(2,1)} %param.20) | copy-start | bytes 3145732
  23.3 0.7 copy-start.8
  24.0 0.7 copy-start.12
  24.0 5.1 %copy-start.4 = (bf16[512,512]{1,0:T(8,128)(2,1)S(1)}, bf16[512,512]{1,0:T(8,128)(2,1)}, u32[]{:S(2)}) copy-start(bf16[512,512]{1,0:T(8,128)(2,1)} %param.26) | copy-start | bytes 1572868
  24.4 31.0 %copy-start.3 = (bf16[1,1024,512]{2,1,0:T(8,128)(2,1)S(1)}, bf16[1,1024,512]{2,1,0:T(8,128)(2,1)}, u32[]{:S(2)}) copy-start(bf16[1,1024,512]{2,1,0:T(8,128)(2,1)} %param.30) | copy-start | bytes 3145732
  58.2 0.7 copy-start.6
  69.6 13.5 %all-to-all-start.2 = ((bf16[16,6,512]{2,1,0:T(8,128)(2,1)}), bf16[16,6,512]{2,1,0:T(8,128)(2,1)S(1)}, u32[]{:S(2)}, u32[]{:S(2)}) async-start(bf16[16,6,512]{2,1,0:T(8,128)(2,1)} %copy.61), calls=%async_computation.3 | async-start | bytes 262144 | tf_op jit(solution)/shard_map/all_to_all | solution.py:144
  75.3 0.7 copy-start.10
Sparse Core Ops, SparseCore 0:
  58.3 9.6 reduce-scatter.1
where the time goes:
time: 96.8 us; the launch traced here: 96.1 us
  blocking collectives  40.4 us (42%)
  waiting for transfers between devices  15.9 us (16%)
  between operations  13.6 us (14%)
  starting transfers between devices  8.9 us (9%)
  matrix products  7.6 us (8%)
  local copies, waits for them, and re-layouts  6.75 us (7%)
  other arithmetic  2.98 us (3%)
    all_to_all x1, blocking collectives, body(): lax.all_to_all(outgoing, 'ep', split_axis=0, concat_axis=0, tiled=True)  16.2 us
    reduce_scatter x1, waiting for transfers between devices, body(): lax.psum_scatter(terms.astype(jnp.bfloat16), 'tp', scatter_dimension=2, t...  8.86 us
    all_to_all x1, waiting for transfers between devices, body(): lax.all_to_all(answers, 'ep', split_axis=0, concat_axis=0, tiled=True)  7.06 us
    all_to_all x1, starting transfers between devices, body(): lax.all_to_all(answers, 'ep', split_axis=0, concat_axis=0, tiled=True)  5.63 us
    all_gather x1, blocking collectives, body(): group_rows = lax.all_gather(tokens, 'tp', axis=0, tiled=True)  5.56 us
    psum x1, blocking collectives, body(): lax.psum((jnp.sum(summed, axis=1), jnp.sum(summed * summed, axis=1)), 'tp')  4.93 us
    psum x1, blocking collectives, body(): lax.psum((jnp.sum(final, axis=1), jnp.sum(final * final, axis=1)), 'tp')  4.93 us
    all_gather x1, blocking collectives, body(): settled = lax.all_gather(settled_part, 'tp', axis=1, tiled=True)  4.35 us
  transfers between devices with their start and end apart: 3, of which 2 were waited for; matrix products, arithmetic and copies ran while one was open for 4% of the time, Pallas kernels for 0%

commit v1 on v0

v1 whole, which is shorter than its diff:
```python
import jax
import jax.numpy as jnp
from jax import lax
from jax.sharding import PartitionSpec as P

ALPHA = 1.4142135623730951
EPS = 1e-05
THETA = 500000.0
LIMIT = 7.0
SLOPE = 1.702
LANES = 128


def rotate(values, positions):
    half = values.shape[-1] // 2
    freqs = THETA ** (-jnp.arange(half, dtype=jnp.float32) / half)
    angles = positions.astype(jnp.float32)[:, None] * freqs[None, :]
    shape = (angles.shape[0],) + (1,) * (values.ndim - 2) + (half,)
    cosine = jnp.cos(angles).reshape(shape)
    sine = jnp.sin(angles).reshape(shape)
    first = values[..., :half]
    second = values[..., half:]
    return jnp.concatenate(
        [first * cosine - second * sine, second * cosine + first * sine], axis=-1
    )


def norm_rows(summed, gain):
    mean = jnp.mean(summed, axis=-1, keepdims=True)
    center = summed - mean
    spread = jnp.mean(center * center, axis=-1, keepdims=True)
    return center * lax.rsqrt(spread + EPS) * gain


def swap(values):
    return lax.ppermute(values, "tp", [(0, 1), (1, 0)])


def joined(mine, other, rank, axis):
    first = rank == 0
    return jnp.concatenate(
        [jnp.where(first, mine, other), jnp.where(first, other, mine)], axis=axis
    )


def gather_tp(values):
    if lax.axis_size("tp") == 2:
        return joined(values, swap(values), lax.axis_index("tp"), 0)
    return lax.all_gather(values, "tp", axis=0, tiled=True)


def regroup_tp(values, own):
    if lax.axis_size("tp") == 2:
        rank = lax.axis_index("tp")
        other = swap(lax.dynamic_slice_in_dim(values, (1 - rank) * own, own))
        return joined(lax.dynamic_slice_in_dim(values, rank * own, own), other, rank, 1)
    return lax.all_to_all(values, "tp", split_axis=0, concat_axis=1, tiled=True)


def sum_tp(values):
    if lax.axis_size("tp") == 2:
        return values + swap(values.astype(jnp.bfloat16)).astype(jnp.float32)
    return lax.psum(values, "tp")


def body(
    tokens,
    lengths,
    key_cache,
    value_cache,
    query_weight,
    key_weight,
    value_weight,
    lambdas,
    head_gain,
    output_weight,
    norm1_gain,
    routes,
    route_logits,
    gate_weight,
    up_weight,
    down_weight,
    norm2_gain,
):
    bf16 = jnp.bfloat16
    f32 = jnp.float32
    tp_count = lax.axis_size("tp")
    tp_rank = lax.axis_index("tp")
    experts = lax.axis_size("ep")
    ep_rank = lax.axis_index("ep")
    own, width = tokens.shape
    group = own * tp_count
    part = width // tp_count
    heads = lambdas.shape[0]
    head_dim = key_weight.shape[1] // 2
    length = key_cache.shape[1]
    group_rows = gather_tp(tokens)
    query = jnp.dot(group_rows, query_weight, preferred_element_type=f32).reshape(
        group, -1, 2, head_dim
    )
    query = rotate(query, lengths).astype(bf16).reshape(group, -1)
    query = regroup_tp(query, own).reshape(own, heads, 2, head_dim)
    own_lengths = lax.dynamic_slice_in_dim(lengths, tp_rank * own, own)
    new_key = jnp.dot(tokens, key_weight, preferred_element_type=f32).reshape(own, 2, head_dim)
    new_key = rotate(new_key, own_lengths).astype(bf16).reshape(own, 2 * head_dim)
    new_value = jnp.dot(tokens, value_weight, preferred_element_type=f32).astype(bf16)
    scale = head_dim ** (-0.5)
    blank = jnp.zeros((own, heads, head_dim), bf16)
    wide = jnp.concatenate(
        [
            jnp.concatenate([query[:, :, 0], blank], axis=-1),
            jnp.concatenate([blank, query[:, :, 1]], axis=-1),
        ],
        axis=1,
    )
    past = jnp.einsum("bqd,bjd->bqj", wide, key_cache, preferred_element_type=f32) * scale
    live = jnp.arange(length, dtype=jnp.int32)[None, :] < own_lengths[:, None]
    past = jnp.where(live[:, None, :], past, -jnp.inf)
    selfs = jnp.sum(wide.astype(f32) * new_key.astype(f32)[:, None, :], axis=-1) * scale
    top = jnp.maximum(jnp.max(past, axis=-1), selfs)
    past_exp = jnp.exp(past - top[..., None])
    self_exp = jnp.exp(selfs - top)
    total = jnp.sum(past_exp, axis=-1) + self_exp
    past_prob = past_exp / total[..., None]
    self_prob = self_exp / total
    mixing = lambdas[None, :]
    past_weight = (past_prob[:, :heads] - mixing[..., None] * past_prob[:, heads:]).astype(bf16)
    self_weight = (self_prob[:, :heads] - mixing * self_prob[:, heads:]).astype(bf16)
    head_out = jnp.einsum("bhj,bje->bhe", past_weight, value_cache, preferred_element_type=f32)
    head_out = head_out + self_weight.astype(f32)[..., None] * new_value.astype(f32)[:, None, :]
    normed = (
        head_out
        * lax.rsqrt(jnp.mean(head_out * head_out, axis=-1, keepdims=True) + EPS)
        * head_gain
    )
    attended = normed.astype(bf16).reshape(own, -1)
    mix = jnp.dot(gather_tp(attended), output_weight, preferred_element_type=f32)
    column_start = tp_rank * part
    own_columns = lax.dynamic_slice_in_dim(group_rows, column_start, part, 1).astype(f32)
    summed = ALPHA * own_columns + mix
    part_mean = jnp.mean(summed, axis=1, keepdims=True)
    mean_high = part_mean.astype(bf16)
    mean_low = (part_mean - mean_high.astype(f32)).astype(bf16)
    lane = jnp.arange(LANES, dtype=jnp.int32)[None, :]
    extra = jnp.where(lane == 0, mean_high, jnp.where(lane == 1, mean_low, jnp.zeros((), bf16)))
    packed = jnp.concatenate([(summed - part_mean).astype(bf16), extra], axis=1)
    packed = jnp.broadcast_to(packed[None], (experts * tp_count,) + packed.shape)
    packed = lax.all_to_all(packed, ("ep", "tp"), split_axis=0, concat_axis=0, tiled=True)
    packed = packed.reshape(experts, tp_count, group, part + LANES).astype(f32)
    pieces = packed[..., :part] + (packed[..., part] + packed[..., part + 1])[..., None]
    everyone = jnp.concatenate([pieces[:, index] for index in range(tp_count)], axis=-1)
    settled = norm_rows(everyone, norm1_gain).astype(bf16)
    rows = settled.reshape(experts * group, width)
    gate_h = jnp.dot(rows, gate_weight[0], preferred_element_type=f32)
    up_h = jnp.dot(rows, up_weight[0], preferred_element_type=f32)
    clipped = jnp.minimum(gate_h, LIMIT)
    linear = jnp.clip(up_h, -LIMIT, LIMIT)
    act = (clipped * jax.nn.sigmoid(SLOPE * clipped) * (linear + 1.0)).astype(bf16)
    terms = jnp.dot(act, down_weight[0], preferred_element_type=f32).astype(bf16)
    terms = terms.reshape(experts, group, width)
    back = lax.all_to_all(terms, "ep", split_axis=0, concat_axis=0, tiled=True)
    route_weight = jax.nn.softmax(route_logits, axis=-1)
    names = jnp.arange(experts, dtype=jnp.int32)[:, None, None]
    dense = jnp.sum(jnp.where(routes[None] == names, route_weight[None], 0.0), axis=-1)
    routed = sum_tp(jnp.sum(back.astype(f32) * dense[:, :, None], axis=0))
    own_settled = lax.dynamic_index_in_dim(settled, ep_rank, 0, keepdims=False)
    final = ALPHA * own_settled.astype(f32) + routed
    mean = jnp.mean(final, axis=-1, keepdims=True)
    spread = jnp.mean((final - mean) * (final - mean), axis=-1, keepdims=True)
    own_final = lax.dynamic_slice_in_dim(final, column_start, part, 1)
    gain = lax.dynamic_slice_in_dim(norm2_gain, column_start, part)
    return ((own_final - mean) * lax.rsqrt(spread + EPS) * gain).astype(bf16)


def solution(mesh):
    in_specs = (
        P(("ep", "tp"), None),
        P("ep"),
        P(("ep", "tp"), None, None),
        P(("ep", "tp"), None, None),
        P(None, "tp"),
        P(),
        P(),
        P(),
        P(),
        P(None, "tp"),
        P(),
        P("ep", None),
        P("ep", None),
        P("ep", None, "tp"),
        P("ep", None, "tp"),
        P("ep", "tp", None),
        P(),
    )
    out_specs = P("ep", "tp")
    return jax.shard_map(body, mesh=mesh, in_specs=in_specs, out_specs=out_specs, check_vma=False)
```

time: 96.8 us -> 61.9 us (0.64)
  blocking collectives: 40.4 us -> 16.4 us
  between operations: 13.6 us -> 0.24 us
  other arithmetic: 2.98 us -> 7.36 us
  local copies, waits for them, and re-layouts: 6.75 us -> 4.51 us
  waiting for transfers between devices: 15.9 us -> 17.2 us
    all_gather x3 -> x0, blocking collectives: 14.3 us -> none  [the longest x1 5.56 us: body(): group_rows = lax.all_gather(tokens, 'tp', axis=0, tiled=True)]
    psum x2 -> x0, blocking collectives: 9.87 us -> none  [the longest x1 4.93 us: body(): lax.psum((jnp.sum(summed, axis=1), jnp.sum(summed * summed, axis=1)), 'tp')]
    ppermute x0 -> x4, waiting for transfers between devices: none -> 9.32 us  [swap(): return lax.ppermute(values, 'tp', [(0, 1), (1, 0)])]
    reduce_scatter x1 -> x0, waiting for transfers between devices: 8.86 us -> none  [body(): lax.psum_scatter(terms.astype(jnp.bfloat16), 'tp', scatter_dimension=2, t...]
    all_to_all x2 -> x1, starting transfers between devices: 8.86 us -> 3.66 us  [body(): back = lax.all_to_all(terms, 'ep', split_axis=0, concat_axis=0, tiled=True)]
    ppermute x0 -> x4, starting transfers between devices: none -> 4.6 us  [swap(): return lax.ppermute(values, 'tp', [(0, 1), (1, 0)])]
    reduce_sum x3 -> x7, other arithmetic: 0.48 us -> 2.51 us  [the longest x1 0.95 us: body(): mean = jnp.mean(final, axis=-1, keepdims=True)]
    reduce_scatter x1 -> x0, local copies, waits for them, and re-layouts: 1.59 us -> none  [body(): lax.psum_scatter(terms.astype(jnp.bfloat16), 'tp', scatter_dimension=2, t...]
  transfers between devices with their start and end apart: 3 -> 5, of which waited for: 2 -> 4; matrix products, arithmetic and copies ran while one was open for 4% -> 8% of each run, Pallas kernels for 0% -> 0%
where the time goes in v1:
time: 61.9 us; the launch traced here: 61.2 us
  waiting for transfers between devices  17.2 us (28%)
  blocking collectives  16.4 us (26%)
  starting transfers between devices  8.26 us (13%)
  other arithmetic  7.36 us (12%)
  matrix products  7.25 us (12%)
  local copies, waits for them, and re-layouts  4.51 us (7%)
    all_to_all x1, blocking collectives, body(): lax.all_to_all(packed, ('ep', 'tp'), split_axis=0, concat_axis=0, tiled=T...  16.4 us
    ppermute x4, waiting for transfers between devices, swap(): return lax.ppermute(values, 'tp', [(0, 1), (1, 0)])  9.32 us
    all_to_all x1, waiting for transfers between devices, body(): back = lax.all_to_all(terms, 'ep', split_axis=0, concat_axis=0, tiled=True)  7.88 us
    ppermute x4, starting transfers between devices, swap(): return lax.ppermute(values, 'tp', [(0, 1), (1, 0)])  4.6 us
    all_to_all x1, starting transfers between devices, body(): back = lax.all_to_all(terms, 'ep', split_axis=0, concat_axis=0, tiled=True)  3.66 us
    unnamed x26, local copies, waits for them, and re-layouts  3.36 us
    dot_general x1, matrix products, body(): jnp.dot(act, down_weight[0], preferred_element_type=f32).astype(bf16)  2.54 us
    convert_element_type x2, other arithmetic, rotate(): angles = positions.astype(jnp.float32)[:, None] * freqs[None, :]  1.39 us
  transfers between devices with their start and end apart: 5, of which 4 were waited for; matrix products, arithmetic and copies ran while one was open for 8% of the time, Pallas kernels for 0%

profile of v1, /device:TPU:0, one launch (start us, length us, event | category | flops | bytes accessed | tf_op | source)
XLA Modules:
  0.0 61.2 jit_solution(6487244251224465581)
XLA Ops:
  0.0 3.0 %collective-permute-start = (bf16[4,1024]{1,0:T(4,128)(2,1)}, bf16[4,1024]{1,0:T(4,128)(2,1)S(1)}, u32[]{:S(2)}, u32[]{:S(2)}) collective-permute-start(bf16[4,1024]{1,0:T(4,128)(2,1)} %param.17), channel_id=1, source_target_pairs={{0,1},{1,0},{2,3},{3,2},{4,5},{5,4},{6,7},{7,6},{8,9},{9,8},{10,11... | collective-permute-start | bytes 24584 | tf_op jit(solution)/shard_map/ppermute | solution.py:36
  3.1 1.1 %fusion.5 = f32[4,128]{1,0:T(4,128)S(1)} fusion(bf16[4,1024]{1,0:T(4,128)(2,1)} %param.17, bf16[1024,128]{1,0:T(8,128)(2,1)} %param.23), kind=kOutput, calls=%fused_computation.12 | convolution fusion | flops 1049600 | bytes 272384 | tf_op jit(solution)/shard_map/dot_general | solution.py:106
  4.2 0.8 %fusion.65 = f32[4,128]{1,0:T(4,128)S(1)} fusion(bf16[4,1024]{1,0:T(4,128)(2,1)} %param.17, bf16[1024,128]{1,0:T(8,128)(2,1)S(1)} %copy-done.5), kind=kOutput, calls=%fused_computation.134 | convolution fusion | flops 1048576 | bytes 272384 | tf_op jit(solution)/shard_map/dot_general | solution.py:104
  5.1 0.7 %convert_element_type.117 = f32[8]{0:T(128)S(1)} convert(s32[8]{0:T(128)} %param.18) | non-fusion elementwise | flops 8 | bytes 64 | tf_op jit(solution)/shard_map/convert_element_type | solution.py:17
  5.8 0.7 %fusion.61 = (f32[4]{0:T(128)S(1)}, s32[4]{0:T(128)S(1)}) fusion(s32[8]{0:T(128)} %param.18, s32[]{:T(128)S(6)} %select_n.73), kind=kLoop, calls=%fused_computation.130 | loop fusion | flops 4 | bytes 52 | tf_op jit(solution)/shard_map/convert_element_type | solution.py:17
  6.9 0.7 %broadcast_select_fusion = (bf16[4,1024]{1,0:T(4,128)(2,1)S(1)}, bf16[4,1024]{1,0:T(4,128)(2,1)S(1)}) fusion(bf16[4,1024]{1,0:T(4,128)(2,1)S(1)} %collective-permute-done, bf16[4,1024]{1,0:T(4,128)(2,1)} %param.17, pred[]{:T(512)S(6)} %eq.40), kind=kLoop, calls=%fused_computation.80 | loop fusion | flops 8192 | bytes 32769 | tf_op jit(solution)/shard_map/jit(_where)/select_n | solution.py:42
  7.6 1.2 %fusion.32 = f32[8,256]{1,0:T(8,128)S(1)} fusion(bf16[1024,256]{1,0:T(8,128)(2,1)} %param.21, bf16[4,1024]{1,0:T(4,128)(2,1)S(1)} %get-tuple-element.18, bf16[4,1024]{1,0:T(4,128)(2,1)S(1)} %get-tuple-element.19), kind=kOutput, calls=%fused_computation.58 | convolution fusion | flops 4227072 | bytes 548864 | tf_op jit(solution)/shard_map/dot_general | solution.py:98
  9.2 0.2 collective-permute-start.1
  9.6 3.3 %collective-permute-done.1 = bf16[4,256]{1,0:T(4,128)(2,1)S(1)} collective-permute-done((bf16[4,256]{1,0:T(4,128)(2,1)S(1)}, bf16[4,256]{1,0:T(4,128)(2,1)S(1)}, u32[]{:S(2)}, u32[]{:S(2)}) %collective-permute-start.1) | collective-permute-done | bytes 2080 | tf_op jit(solution)/shard_map/ppermute | solution.py:36
  13.1 0.5 fusion.63
  13.6 0.2 fusion.25
  14.0 0.6 %copy-done.9 = f32[4]{0:T(128)S(1)} copy-done((f32[4]{0:T(128)S(1)}, f32[4]{0:T(128)}, u32[]{:S(2)}) %copy-start.9) | copy-done | bytes 40
  14.7 0.4 multiply_reduce_fusion.4
  15.1 0.7 %copy-done.11 = f32[128]{0:T(128)S(1)} copy-done((f32[128]{0:T(128)S(1)}, f32[128]{0:T(128)}, u32[]{:S(2)}) %copy-start.11) | copy-done | bytes 536
  15.8 0.2 collective-permute-start.2
  16.0 3.4 %collective-permute-done.2 = bf16[4,512]{1,0:T(4,128)(2,1)S(1)} collective-permute-done((bf16[4,512]{1,0:T(4,128)(2,1)S(1)}, bf16[4,512]{1,0:T(4,128)(2,1)S(1)}, u32[]{:S(2)}, u32[]{:S(2)}) %collective-permute-start.2) | collective-permute-done | bytes 4128 | tf_op jit(solution)/shard_map/ppermute | solution.py:36
  19.5 0.3 fusion.64
  20.0 16.4 %all_to_all.10 = bf16[32,8,640]{2,1,0:T(8,128)(2,1)S(1)} all-to-all(bf16[32,8,640]{2,1,0:T(8,128)(2,1)S(1)} %broadcast_in_dim.65), channel_id=1, replica_groups=mesh['ep'=16,'tp'=2] {'ep','tp'}, dimensions={0} | all-to-all | bytes 655360 | tf_op jit(solution)/shard_map/all_to_all | solution.py:148
  37.3 0.9 %multiply_reduce_fusion.1 = (f32[16,8]{1,0:T(8,128)S(1)}, f32[16,8,1024]{2,1,0:T(8,128)}) fusion(f32[16,8]{1,0:T(8,128)S(1)} %add_multiply_fusion, f32[16,8,512]{2,1,0:T(8,128)S(1)} %get-tuple-element.15, f32[16,8,512]{2,1,0:T(8,128)S(1)} %get-tuple-element.11), kind=kLoop, calls=%fused_computation.23 | loop fusion | flops 524160 | bytes 1049600 | tf_op jit(solution)/shard_map/reduce_sum | solution.py:31
  38.3 0.6 copy-done.7
  38.9 0.4 convolution_minimum_fusion
  39.3 2.5 %fusion = bf16[16,8,1024]{2,1,0:T(8,128)(2,1)} fusion(bf16[1,512,1024]{2,1,0:T(8,128)(2,1)S(1)} %copy-done, bf16[1,1024,512]{2,1,0:T(8,128)(2,1)} %param.31, f32[128,512]{1,0:T(8,128)S(1)} %convolution_minimum_fusion, f32[128,512]{1,0:T(8,128)S(1)} %get-tuple-element.14, f32[128,512]{1,0:T(8,128)S(1)} %get-tuple-element.12, f32[1024]{0:T(1024)S(1)} %copy-done.7, ...), kind=kOutput, calls=%fused_computation.1 | convolution fusion | flops 269811712 | bytes 3150848 | tf_op jit(solution)/shard_map/dot_general | solution.py:159
  41.8 3.7 %all-to-all-start.1 = ((bf16[16,8,1024]{2,1,0:T(8,128)(2,1)}), bf16[16,8,1024]{2,1,0:T(8,128)(2,1)S(1)}, u32[]{:S(2)}, u32[]{:S(2)}) async-start(bf16[16,8,1024]{2,1,0:T(8,128)(2,1)} %fusion), calls=%async_computation.1 | async-start | bytes 524288 | tf_op jit(solution)/shard_map/all_to_all | solution.py:161
  45.6 0.2 fusion.42
  46.0 0.6 %copy-done.8 = s32[8,6]{1,0:T(8,128)S(1)} copy-done((s32[8,6]{1,0:T(8,128)S(1)}, s32[8,6]{1,0:T(8,128)}, u32[]{:S(2)}) %copy-start.8) | copy-done | bytes 216
  46.8 0.7 %copy-done.10 = f32[1024]{0:T(1024)S(1)} copy-done((f32[1024]{0:T(1024)S(1)}, f32[1024]{0:T(1024)}, u32[]{:S(2)}) %copy-start.10) | copy-done | bytes 4120
  47.6 7.9 %all-to-all-done.1 = bf16[16,8,1024]{2,1,0:T(8,128)(2,1)S(1)} async-done(((bf16[16,8,1024]{2,1,0:T(8,128)(2,1)}), bf16[16,8,1024]{2,1,0:T(8,128)(2,1)S(1)}, u32[]{:S(2)}, u32[]{:S(2)}) %all-to-all-start.1) | async-done | bytes 262176 | tf_op jit(solution)/shard_map/all_to_all | solution.py:161
  55.6 1.2 %collective-permute-start.3 = (bf16[8,1024]{1,0:T(8,128)(2,1)S(1)}, bf16[8,1024]{1,0:T(8,128)(2,1)S(1)}, u32[]{:S(2)}, u32[]{:S(2)}) collective-permute-start(bf16[8,1024]{1,0:T(8,128)(2,1)S(1)} %convert_element_type.141), channel_id=1, source_target_pairs={{0,1},{1,0},{2,3},{3,2},{4,5},{5,4},{6,7},{7,6},{8,9},{9,8},{10,11... | collective-permute-start | bytes 49160 | tf_op jit(solution)/shard_map/ppermute | solution.py:36
  56.8 2.6 %collective-permute-done.3 = bf16[8,1024]{1,0:T(8,128)(2,1)S(1)} collective-permute-done((bf16[8,1024]{1,0:T(8,128)(2,1)S(1)}, bf16[8,1024]{1,0:T(8,128)(2,1)S(1)}, u32[]{:S(2)}, u32[]{:S(2)}) %collective-permute-start.3) | collective-permute-done | bytes 16416 | tf_op jit(solution)/shard_map/ppermute | solution.py:36
  59.4 0.9 %fusion.60 = (f32[8]{0:T(128)S(1)}, f32[8,1024]{1,0:T(8,128)S(1)}) fusion(f32[8,1024]{1,0:T(8,128)S(1)} %multiply_reduce_fusion, bf16[8,1024]{1,0:T(8,128)(2,1)S(1)} %collective-permute-done.3, f32[1024]{0:T(1024)S(1)} %copy-done.7, f32[1,8]{1,0:T(1,128)S(1)} %constant_dynamic-slice_fusion, f32[16,8,1024]{2,1,0:T(8,128)} %get-tuple-element.8, s32[]{:T(128)S(6)} %select_n.83), kind=kLoop, calls=%fused_computation.129 | loop fusion | flops 73720 | bytes 118852 | tf_op jit(solution)/shard_map/reduce_sum | solution.py:168
  60.4 0.2 multiply_reduce_fusion.2
  60.6 0.7 %multiply_convert_fusion = bf16[8,512]{1,0:T(8,128)(2,1)} fusion(f32[8,1024]{1,0:T(8,128)S(1)} %get-tuple-element.6, s32[]{:T(128)S(6)} %select_n.71, f32[512]{0:T(512)S(1)} %dynamic_slice.28, f32[8]{0:T(128)S(1)} %add_rsqrt_fusion.2, f32[8]{0:T(128)S(1)} %broadcast_multiply_fusion), kind=kLoop, calls=%fused_computation.61 | loop fusion | flops 16384 | bytes 26692 | tf_op jit(solution)/shard_map/convert_element_type | solution.py:172
  (76 shorter events, 3.4 us)
Async XLA Ops:
  0.0 39.3 %copy-start = (bf16[1,512,1024]{2,1,0:T(8,128)(2,1)S(1)}, bf16[1,512,1024]{2,1,0:T(8,128)(2,1)}, u32[]{:S(2)}) copy-start(bf16[1,512,1024]{2,1,0:T(8,128)(2,1)} %param.32) | copy-start | bytes 3145732
  0.0 4.2 %copy-start.5 = (bf16[1024,128]{1,0:T(8,128)(2,1)S(1)}, bf16[1024,128]{1,0:T(8,128)(2,1)}, u32[]{:S(2)}) copy-start(bf16[1024,128]{1,0:T(8,128)(2,1)} %param.22) | copy-start | bytes 786436
  0.0 13.1 %copy-start.1 = (bf16[4,1024,128]{2,1,0:T(8,128)(2,1)S(1)}, bf16[4,1024,128]{2,1,0:T(8,128)(2,1)}, u32[]{:S(2)}) copy-start(bf16[4,1024,128]{2,1,0:T(8,128)(2,1)} %param.19) | copy-start | bytes 3145732
  0.0 6.9 %collective-permute-start = (bf16[4,1024]{1,0:T(4,128)(2,1)}, bf16[4,1024]{1,0:T(4,128)(2,1)S(1)}, u32[]{:S(2)}, u32[]{:S(2)}) collective-permute-start(bf16[4,1024]{1,0:T(4,128)(2,1)} %param.17), channel_id=1, source_target_pairs={{0,1},{1,0},{2,3},{3,2},{4,5},{5,4},{6,7},{7,6},{8,9},{9,8},{10,11... | collective-permute-start | bytes 24584 | tf_op jit(solution)/shard_map/ppermute | solution.py:36
  8.8 5.9 %copy-start.2 = (bf16[4,1024,128]{2,1,0:T(8,128)(2,1)S(1)}, bf16[4,1024,128]{2,1,0:T(8,128)(2,1)}, u32[]{:S(2)}) copy-start(bf16[4,1024,128]{2,1,0:T(8,128)(2,1)} %param.20) | copy-start | bytes 3145732
  9.2 3.6 %collective-permute-start.1 = (bf16[4,256]{1,0:T(4,128)(2,1)S(1)}, bf16[4,256]{1,0:T(4,128)(2,1)S(1)}, u32[]{:S(2)}, u32[]{:S(2)}) collective-permute-start(bf16[4,256]{1,0:T(4,128)(2,1)S(1)} %constant_dynamic-slice_fusion.1), channel_id=1, source_target_pairs={{0,1},{1,0},{2,3},{3,2},{4,5},{5,4},{6,7},{7,6},{8,9},{9,8},{10,11... | collective-permute-start | bytes 6152 | tf_op jit(solution)/shard_map/ppermute | solution.py:36
  14.0 0.7 %copy-start.9 = (f32[4]{0:T(128)S(1)}, f32[4]{0:T(128)}, u32[]{:S(2)}) copy-start(f32[4]{0:T(128)} %param.24) | copy-start | bytes 52
  14.7 4.8 %copy-start.4 = (bf16[512,512]{1,0:T(8,128)(2,1)S(1)}, bf16[512,512]{1,0:T(8,128)(2,1)}, u32[]{:S(2)}) copy-start(bf16[512,512]{1,0:T(8,128)(2,1)} %param.26) | copy-start | bytes 1572868
  15.1 0.7 %copy-start.11 = (f32[128]{0:T(128)S(1)}, f32[128]{0:T(128)}, u32[]{:S(2)}) copy-start(f32[128]{0:T(128)} %param.25) | copy-start | bytes 1540
  15.8 3.6 %collective-permute-start.2 = (bf16[4,512]{1,0:T(4,128)(2,1)S(1)}, bf16[4,512]{1,0:T(4,128)(2,1)S(1)}, u32[]{:S(2)}, u32[]{:S(2)}) collective-permute-start(bf16[4,512]{1,0:T(4,128)(2,1)S(1)} %bitcast.54), channel_id=1, source_target_pairs={{0,1},{1,0},{2,3},{3,2},{4,5},{5,4},{6,7},{7,6},{8,9},{9,8},{10,11... | collective-permute-start | bytes 12296 | tf_op jit(solution)/shard_map/ppermute | solution.py:36
  37.1 1.2 %copy-start.3 = (bf16[1,1024,512]{2,1,0:T(8,128)(2,1)S(1)}, bf16[1,1024,512]{2,1,0:T(8,128)(2,1)}, u32[]{:S(2)}) copy-start(bf16[1,1024,512]{2,1,0:T(8,128)(2,1)} %param.30) | copy-start | bytes 3145732
  38.2 0.7 %copy-start.7 = (f32[1024]{0:T(1024)S(1)}, f32[1024]{0:T(1024)}, u32[]{:S(2)}) copy-start(f32[1024]{0:T(1024)} %param.27) | copy-start | bytes 12292
  41.8 3.7 %copy-start.6 = (f32[8,6]{1,0:T(8,128)S(1)}, f32[8,6]{1,0:T(8,128)}, u32[]{:S(2)}) copy-start(f32[8,6]{1,0:T(8,128)} %param.29) | copy-start | bytes 580
  41.8 13.6 %all-to-all-start.1 = ((bf16[16,8,1024]{2,1,0:T(8,128)(2,1)}), bf16[16,8,1024]{2,1,0:T(8,128)(2,1)S(1)}, u32[]{:S(2)}, u32[]{:S(2)}) async-start(bf16[16,8,1024]{2,1,0:T(8,128)(2,1)} %fusion), calls=%async_computation.1 | async-start | bytes 524288 | tf_op jit(solution)/shard_map/all_to_all | solution.py:161
  45.9 0.7 %copy-start.8 = (s32[8,6]{1,0:T(8,128)S(1)}, s32[8,6]{1,0:T(8,128)}, u32[]{:S(2)}) copy-start(s32[8,6]{1,0:T(8,128)} %param.28) | copy-start | bytes 580
  46.8 0.7 %copy-start.10 = (f32[1024]{0:T(1024)S(1)}, f32[1024]{0:T(1024)}, u32[]{:S(2)}) copy-start(f32[1024]{0:T(1024)} %param.33) | copy-start | bytes 12292
  55.6 3.8 %collective-permute-start.3 = (bf16[8,1024]{1,0:T(8,128)(2,1)S(1)}, bf16[8,1024]{1,0:T(8,128)(2,1)S(1)}, u32[]{:S(2)}, u32[]{:S(2)}) collective-permute-start(bf16[8,1024]{1,0:T(8,128)(2,1)S(1)} %convert_element_type.141), channel_id=1, source_target_pairs={{0,1},{1,0},{2,3},{3,2},{4,5},{5,4},{6,7},{7,6},{8,9},{9,8},{10,11... | collective-permute-start | bytes 49160 | tf_op jit(solution)/shard_map/ppermute | solution.py:36
